TPU v7x, 32 devices: a whole 2x2x4 slice. The times are simulated.
32 devices in a mesh: sp: 8 (over z, y), tp: 4 (over x, core).
Axes of the slice: x: 2, y: 2, z: 4, core: 2. Of those that a mesh axis runs over, the one named last changes fastest.
Arguments:
- tokens: bfloat16 [1024, 2048], P(('sp', 'tp')), may hold values from -70 to 70
- w_query: bfloat16 [2048, 2048], P(None, 'tp'), may hold values from -0.1875 to 0.1875
- w_key: bfloat16 [2048, 1024], P(None, 'tp'), may hold values from -0.1875 to 0.1875
- w_value: bfloat16 [2048, 1024], P(None, 'tp'), may hold values from -0.125 to 0.125
- w_out: bfloat16 [2048, 2048], P('tp'), may hold values from -0.125 to 0.125
- lambda_head: float32 [16], P('tp'), may hold values from 0.3 to 0.8
- sub_gain: float32 [128], replicated, may hold values from 0.1 to 1.9
Outputs:
- mixed_rows: bfloat16 [1024, 2048], P(('sp', 'tp'))
All inputs are finite; a program needn't handle non-finite values.
Results may differ from a plain program's by a relative error of at most 0.015.
The roundings to bfloat16 on the way count: a program that leaves them out, or rounds other values in their place, can miss the bound.
Values may be sent and summed in bfloat16 or wider, within the bound.
A program may use at most 64 MiB of HBM per device.

v0:
```python
import functools
import math

import jax
import jax.numpy as jnp
from jax import lax
from jax.experimental import pallas as pl
from jax.experimental.pallas import tpu as pltpu
from jax.sharding import PartitionSpec as P

QK = 64
VD = 128
MESH = pl.DeviceIdType.MESH
F32 = jnp.float32
BF16 = jnp.bfloat16


def kernel(
    sp_size,
    tp_size,
    tok_hbm,
    wq_hbm,
    wk_hbm,
    wv_hbm,
    wo_hbm,
    lam_ref,
    gain_ref,
    out_ref,
    tok,
    wq,
    wk,
    wv,
    wo,
    kv,
    q_t,
    acc,
    peak,
    total,
    heads,
    part,
    from_sib,
    pair_out,
    pair_in,
    load_sem,
    tok_send,
    tok_fwd,
    tok_recv,
    kv_next,
    kv_side,
    kv_recv,
    sib_send,
    sib_recv,
    pair_send,
    pair_recv,
):
    pairs = tp_size // 2
    rows = tok.shape[2]
    depth = tok.shape[3]
    count = pairs * 2 * rows
    key_cols = wk.shape[1]
    groups = key_cols // (2 * QK)
    subs = 2 * groups
    chunks, width = part.shape[0], part.shape[4]

    sp = lax.axis_index("sp")
    tp = lax.axis_index("tp")
    pair = tp // 2
    core = lax.rem(tp, 2)
    sibling = tp + 1 - 2 * core
    inner = lax.rem(sp, 2)
    outer = sp // 2
    side = sp + 1 - 2 * inner
    has_next = sp + 2 < sp_size
    has_prev = sp >= 2

    def far(step):
        return lax.rem(pair + step, pairs)

    def near(step):
        return lax.rem(pair + pairs - step, pairs)

    load_tok = pltpu.make_async_copy(tok_hbm, tok.at[pair, core], load_sem.at[0])
    load_wk = pltpu.make_async_copy(wk_hbm, wk, load_sem.at[1])
    load_wv = pltpu.make_async_copy(wv_hbm, wv, load_sem.at[2])
    load_wq = pltpu.make_async_copy(wq_hbm, wq, load_sem.at[3])
    load_wo = pltpu.make_async_copy(wo_hbm, wo, load_sem.at[4])
    for load in (load_tok, load_wk, load_wv, load_wq, load_wo):
        load.start()

    barrier = pltpu.get_barrier_semaphore()
    pl.semaphore_signal(barrier, inc=1, device_id={"tp": sibling}, device_id_type=MESH)
    for step in range(1, pairs):
        pl.semaphore_signal(
            barrier, inc=1, device_id={"tp": far(step) * 2 + core}, device_id_type=MESH
        )
    pl.semaphore_signal(barrier, inc=1, device_id={"sp": side}, device_id_type=MESH)

    @pl.when(has_next)
    def _():
        pl.semaphore_signal(barrier, inc=1, device_id={"sp": sp + 2}, device_id_type=MESH)

    @pl.when(has_prev)
    def _():
        pl.semaphore_signal(barrier, inc=1, device_id={"sp": sp - 2}, device_id_type=MESH)

    pl.semaphore_wait(barrier, 1 + pairs + has_next.astype(jnp.int32) + has_prev.astype(jnp.int32))

    def tok_copy(slot_pair, slot_core, sem, device):
        slot = tok.at[slot_pair, slot_core]
        return pltpu.make_async_remote_copy(
            src_ref=slot,
            dst_ref=slot,
            send_sem=sem,
            recv_sem=tok_recv.at[slot_pair, slot_core],
            device_id={"tp": device},
            device_id_type=MESH,
        )

    load_tok.wait()
    far_sends = [
        tok_copy(pair, core, tok_send.at[step], far(step) * 2 + core) for step in range(1, pairs)
    ]
    own_send = tok_copy(pair, core, tok_send.at[0], sibling)
    for copy in far_sends:
        copy.start()
    own_send.start()

    def kv_copy(block, chunk, sub, sems, device):
        slot = kv.at[block, chunk, sub]
        return pltpu.make_async_remote_copy(
            src_ref=slot,
            dst_ref=slot,
            send_sem=sems.at[block, chunk, sub],
            recv_sem=kv_recv.at[block, chunk, sub],
            device_id={"sp": device},
            device_id_type=MESH,
        )

    def pass_on(block, chunk, sub):
        @pl.when(has_next)
        def _():
            kv_copy(block, chunk, sub, kv_next, sp + 2).start()

        @pl.when(block < side)
        def _():
            kv_copy(block, chunk, sub, kv_side, side).start()

    def sent(block, chunk, sub):
        @pl.when(has_next)
        def _():
            kv_copy(block, chunk, sub, kv_next, sp + 2).wait_send()

        @pl.when(block < side)
        def _():
            kv_copy(block, chunk, sub, kv_side, side).wait_send()

    def arrived(block, chunk, sub):
        kv_copy(block, chunk, sub, kv_side, side).wait_recv()

    def relay(block, step):
        for sub in range(subs):
            arrived(block, near(step), sub)
            pass_on(block, near(step), sub)

    def project(chunk):
        x = tok[chunk].reshape(2 * rows, depth)
        for first, weight in ((0, wk), (groups, wv)):
            made = jnp.dot(x, weight[...], preferred_element_type=F32).astype(BF16)
            for g in range(groups):
                kv[sp, chunk, first + g] = made[:, g * VD : (g + 1) * VD]
                pass_on(sp, chunk, first + g)

    gain_t = jnp.broadcast_to(gain_ref[...], (count, VD)).T

    tok_copy(pair, 1 - core, tok_send.at[0], sibling).wait_recv()
    load_wk.wait()
    load_wv.wait()
    project(pair)
    fwds = []
    for step in range(1, pairs):
        source = near(step)
        tok_copy(source, core, tok_send.at[0], sibling).wait_recv()
        fwd = tok_copy(source, core, tok_fwd.at[step], sibling)
        fwd.start()
        fwds.append(fwd)

    @pl.when(has_prev)
    def _():
        relay(sp - 2, 0)

    for step in range(1, pairs):
        source = near(step)
        tok_copy(source, 1 - core, tok_send.at[0], sibling).wait_recv()
        project(source)

    load_wq.wait()
    queries = jnp.dot(tok[...].reshape(count, depth), wq[...], preferred_element_type=F32)
    queries = queries.astype(BF16).astype(F32) * (1.0 / math.sqrt(QK))
    map_of = lax.broadcasted_iota(jnp.int32, (2 * QK, count), 0) // QK
    for g in range(groups):
        for k in range(2):
            at = (g * 2 + k) * 2 * QK
            turned = queries[:, at : at + 2 * QK].T
            for m in range(2):
                q_t[g, :, pl.ds((k * 2 + m) * count, count)] = jnp.where(
                    map_of == m, turned, 0.0
                ).astype(BF16)

    wide = 4 * count

    def absorb(block, first):
        for g in range(groups):
            keys = kv[block, :, g].reshape(count, 2 * QK)
            values = kv[block, :, groups + g].reshape(count, VD)
            scores = jnp.dot(keys, q_t[g], preferred_element_type=F32)
            if first:
                key_at = lax.broadcasted_iota(jnp.int32, (count, wide), 0)
                query_at = lax.rem(lax.broadcasted_iota(jnp.int32, (count, wide), 1), count)
                scores = jnp.where(key_at <= query_at, scores, -jnp.inf)
            top = jnp.max(scores, axis=0, keepdims=True)
            if not first:
                old = peak[g]
                top = jnp.maximum(top, old)
                fade = jnp.exp(old - top)
            expo = jnp.exp(scores - top)
            amount = jnp.sum(expo, axis=0, keepdims=True)
            summed = lax.dot_general(
                values, expo.astype(BF16), (((0,), (0,)), ((), ())), preferred_element_type=F32
            )
            if not first:
                amount = amount + total[g] * fade
                summed = summed + acc[g] * fade
            peak[g] = top
            total[g] = amount
            acc[g] = summed

    absorb(sp, True)

    def turn(d, carried):
        block = sp - 2 * d

        @pl.when(d < outer)
        def _():
            relay(block - 2, 0)

        for step in range(1, pairs):
            relay(block, step)
        absorb(block, False)
        return carried

    lax.fori_loop(1, outer + 1, turn, 0)

    def beside(d, carried):
        block = side - 2 * d
        for step in range(pairs):
            for sub in range(subs):
                arrived(block, near(step), sub)
        absorb(block, False)
        return carried

    lax.fori_loop(1 - inner, outer + 1, beside, 0)

    for g in range(groups):
        for k in range(2):
            left = pl.ds((k * 2) * count, count)
            right = pl.ds((k * 2 + 1) * count, count)
            mixed = acc[g, :, left] / total[g, :, left] - lam_ref[g * 2 + k] * (
                acc[g, :, right] / total[g, :, right]
            )
            power = jnp.mean(mixed * mixed, axis=0, keepdims=True)
            head = mixed * lax.rsqrt(power + 1e-6) * gain_t
            heads[:, (g * 2 + k) * VD : (g * 2 + k + 1) * VD] = head.T.astype(BF16)

    load_wo.wait()

    def sib_copy(j):
        return pltpu.make_async_remote_copy(
            src_ref=part.at[j, 1 - core],
            dst_ref=from_sib.at[j],
            send_sem=sib_send.at[j],
            recv_sem=sib_recv.at[j],
            device_id={"tp": sibling},
            device_id_type=MESH,
        )

    def pair_copy(j, step):
        return pltpu.make_async_remote_copy(
            src_ref=pair_out.at[j, step],
            dst_ref=pair_in.at[j, step],
            send_sem=pair_send.at[j, step],
            recv_sem=pair_recv.at[j, step],
            device_id={"tp": far(step) * 2 + core},
            device_id_type=MESH,
        )

    for j in range(chunks):
        partial = jnp.dot(
            heads[...], wo[:, j * width : (j + 1) * width], preferred_element_type=F32
        ).astype(BF16)
        for p in range(pairs):
            for c in range(2):
                at = (p * 2 + c) * rows
                part[j, c, p] = partial[at : at + rows]
        sib_copy(j).start()
    for j in range(chunks):
        sib_copy(j).wait_recv()
        for step in range(1, pairs):
            goal = far(step)
            pair_out[j, step] = (
                part[j, core, goal].astype(F32) + from_sib[j, goal].astype(F32)
            ).astype(BF16)
            pair_copy(j, step).start()
    for j in range(chunks):
        result = part[j, core, pair].astype(F32) + from_sib[j, pair].astype(F32)
        for step in range(1, pairs):
            pair_copy(j, step).wait_recv()
            result = result + pair_in[j, step].astype(F32)
        out_ref[:, j * width : (j + 1) * width] = result.astype(BF16)

    own_send.wait_send()
    for copy in far_sends + fwds:
        copy.wait_send()

    def drain(d, carried):
        for step in range(pairs):
            for sub in range(subs):
                sent(sp - 2 * d, near(step), sub)
        return carried

    lax.fori_loop(0, outer + 1, drain, 0)
    for j in range(chunks):
        sib_copy(j).wait_send()
        for step in range(1, pairs):
            pair_copy(j, step).wait_send()


def body(sp_size, tp_size, tokens, w_query, w_key, w_value, w_out, lambda_head, sub_gain):
    rows, depth = tokens.shape
    pairs = tp_size // 2
    count = rows * tp_size
    key_cols = w_key.shape[1]
    groups = key_cols // (2 * QK)
    subs = 2 * groups
    out_cols = w_out.shape[1]
    chunks = math.gcd(out_cols // 128, 4)
    width = out_cols // chunks
    anywhere = pl.BlockSpec(memory_space=pl.ANY)
    dma = pltpu.SemaphoreType.DMA
    return pl.pallas_call(
        functools.partial(kernel, sp_size, tp_size),
        out_shape=jax.ShapeDtypeStruct((rows, out_cols), BF16),
        in_specs=[anywhere] * 5
        + [pl.BlockSpec(memory_space=pltpu.SMEM), pl.BlockSpec(memory_space=pltpu.VMEM)],
        out_specs=pl.BlockSpec(memory_space=pltpu.VMEM),
        scratch_shapes=[
            pltpu.VMEM((pairs, 2, rows, depth), BF16),
            pltpu.VMEM(w_query.shape, BF16),
            pltpu.VMEM(w_key.shape, BF16),
            pltpu.VMEM(w_value.shape, BF16),
            pltpu.VMEM(w_out.shape, BF16),
            pltpu.VMEM((sp_size, pairs, subs, 2 * rows, VD), BF16),
            pltpu.VMEM((groups, 2 * QK, 4 * count), BF16),
            pltpu.VMEM((groups, VD, 4 * count), F32),
            pltpu.VMEM((groups, 1, 4 * count), F32),
            pltpu.VMEM((groups, 1, 4 * count), F32),
            pltpu.VMEM((count, groups * 2 * VD), BF16),
            pltpu.VMEM((chunks, 2, pairs, rows, width), BF16),
            pltpu.VMEM((chunks, pairs, rows, width), BF16),
            pltpu.VMEM((chunks, pairs, rows, width), BF16),
            pltpu.VMEM((chunks, pairs, rows, width), BF16),
            dma((5,)),
            dma((pairs,)),
            dma((pairs,)),
            dma((pairs, 2)),
            dma((sp_size, pairs, subs)),
            dma((sp_size, pairs, subs)),
            dma((sp_size, pairs, subs)),
            dma((chunks,)),
            dma((chunks,)),
            dma((chunks, pairs)),
            dma((chunks, pairs)),
        ],
        compiler_params=pltpu.CompilerParams(
            collective_id=0, has_side_effects=True, vmem_limit_bytes=60 * 1024 * 1024
        ),
    )(tokens, w_query, w_key, w_value, w_out, lambda_head, sub_gain.reshape(1, VD))


def solution(mesh):
    return jax.shard_map(
        functools.partial(body, mesh.shape["sp"], mesh.shape["tp"]),
        mesh=mesh,
        in_specs=(
            P(("sp", "tp"), None),
            P(None, "tp"),
            P(None, "tp"),
            P(None, "tp"),
            P("tp", None),
            P("tp"),
            P(),
        ),
        out_specs=P(("sp", "tp"), None),
        check_vma=False,
    )
```

profile of v0, /device:TPU:25, one launch (start us, length us, event | category | flops | bytes accessed | tf_op | source)
XLA Modules:
  0.0 29.8 jit_solution(4212268678237882057)
XLA Ops:
  0.0 28.2 %shard_map.73 = bf16[32,2048]{1,0:T(8,128)(2,1)} custom-call(bf16[32,2048]{1,0:T(8,128)(2,1)} %tok_hbm.1, bf16[2048,512]{1,0:T(8,128)(2,1)} %wq_hbm.1, bf16[2048,256]{1,0:T(8,128)(2,1)} %wk_hbm.1, bf16[2048,256]{1,0:T(8,128)(2,1)} %wv_hbm.1, bf16[512,2048]{1,0:T(8,128)(2,1)} %wo_hbm.1, f32[4]{0:T(128)} %lam_ref.1, f32[1,128]{1,0:T(1,128)} %bitcast.1), custom_call_target="tpu_custom_call" | custom-call | tf_op jit(solution)/shard_map/pallas_call | solution.py:349
  28.2 1.6 %copy.9 = bf16[32,2048]{1,0:T(8,128)(2,1)} copy(bf16[32,2048]{1,0:T(8,128)(2,1)} %shard_map.73) | data formatting | bytes 262144
where the time goes:
time: 30.2 us; the launch traced here: 29.8 us
  Pallas kernels  28.2 us (93%)
  local copies, waits for them, and re-layouts  1.57 us (5%)
    pallas_call x1, Pallas kernels, body(): pl.pallas_call(functools.partial(kernel, sp_size, tp_size), out_shape=jax...  28.2 us
    unnamed x1, local copies, waits for them, and re-layouts  1.57 us

commit v1 on v0

--- a/solution.py
+++ b/solution.py
@@ -348,7 +348,7 @@
     dma = pltpu.SemaphoreType.DMA
     return pl.pallas_call(
         functools.partial(kernel, sp_size, tp_size),
-        out_shape=jax.ShapeDtypeStruct((rows, out_cols), BF16),
+        out_shape=pltpu.VMEM((rows, out_cols), BF16),
         in_specs=[anywhere] * 5
         + [pl.BlockSpec(memory_space=pltpu.SMEM), pl.BlockSpec(memory_space=pltpu.VMEM)],
         out_specs=pl.BlockSpec(memory_space=pltpu.VMEM),

time: 30.2 us -> 28.7 us (0.950)
  local copies, waits for them, and re-layouts: 1.57 us -> 0.66 us
  Pallas kernels: 28.2 us -> 27.6 us
    unnamed x1, local copies, waits for them, and re-layouts: 1.57 us -> 0.66 us
    pallas_call x1, Pallas kernels: 28.2 us -> 27.6 us  [body(): pl.pallas_call(functools.partial(kernel, sp_size, tp_size), out_shape=plt...]
where the time goes in v1:
time: 28.7 us; the launch traced here: 28.2 us
  Pallas kernels  27.6 us (96%)
  local copies, waits for them, and re-layouts  0.66 us (2%)
    pallas_call x1, Pallas kernels, body(): pl.pallas_call(functools.partial(kernel, sp_size, tp_size), out_shape=plt...  27.6 us
    unnamed x1, local copies, waits for them, and re-layouts  0.66 us

profile of v1, /device:TPU:25, one launch (start us, length us, event | category | flops | bytes accessed | tf_op | source)
XLA Modules:
  0.0 28.2 jit_solution(5159737893863149267)
XLA Ops:
  0.0 27.6 %shard_map.73 = bf16[32,2048]{1,0:T(8,128)(2,1)S(1)} custom-call(bf16[32,2048]{1,0:T(8,128)(2,1)} %tok_hbm.1, bf16[2048,512]{1,0:T(8,128)(2,1)} %wq_hbm.1, bf16[2048,256]{1,0:T(8,128)(2,1)} %wk_hbm.1, bf16[2048,256]{1,0:T(8,128)(2,1)} %wv_hbm.1, bf16[512,2048]{1,0:T(8,128)(2,1)} %wo_hbm.1, f32[4]{0:T(128)} %lam_ref.1, f32[1,128]{1,0:T(1,128)} %bitcast.1), custom_call_target="tpu_custom_call" | custom-call | tf_op jit(solution)/shard_map/pallas_call | solution.py:349
  27.6 0.7 %copy.9 = bf16[32,2048]{1,0:T(8,128)(2,1)} copy(bf16[32,2048]{1,0:T(8,128)(2,1)S(1)} %shard_map.73) | data formatting | bytes 262144

commit v2 on v1

v2 whole, which is shorter than its diff:
```python
import functools
import math

import jax
import jax.numpy as jnp
from jax import lax
from jax.experimental import pallas as pl
from jax.experimental.pallas import tpu as pltpu
from jax.sharding import PartitionSpec as P

QK = 64
VD = 128
MESH = pl.DeviceIdType.MESH
F32 = jnp.float32
BF16 = jnp.bfloat16


def kernel(
    sp_size,
    tp_size,
    tok_hbm,
    wq_hbm,
    wk_hbm,
    wv_hbm,
    wo_hbm,
    lam_ref,
    gain_ref,
    out_ref,
    tok,
    wq,
    wkv,
    wo,
    kv,
    q_t,
    acc,
    peak,
    total,
    heads,
    part,
    from_sib,
    pair_out,
    pair_in,
    load_sem,
    tok_send,
    tok_recv,
    kv_next,
    kv_side,
    kv_recv,
    out_send,
    sib_recv,
    pair_recv,
):
    pairs = tp_size // 2
    half = tok.shape[3]
    rows = 2 * half
    depth = tok.shape[4]
    count = pairs * 2 * rows
    key_cols = wkv.shape[2]
    groups = key_cols // (2 * QK)
    chunks, width = part.shape[0], part.shape[4]

    sp = lax.axis_index("sp")
    tp = lax.axis_index("tp")
    pair = tp // 2
    core = lax.rem(tp, 2)
    sibling = tp + 1 - 2 * core
    inner = lax.rem(sp, 2)
    outer = sp // 2
    side = sp + 1 - 2 * inner
    has_next = sp + 2 < sp_size
    has_prev = sp >= 2

    def far(step):
        return lax.rem(pair + step, pairs)

    def near(step):
        return lax.rem(pair + pairs - step, pairs)

    for h in range(2):
        pltpu.make_async_copy(
            tok_hbm.at[pl.ds(h * half, half)], tok.at[pair, core, h], load_sem.at[0]
        ).start()
    load_tok = pltpu.make_async_copy(tok.at[pair, core], tok.at[pair, core], load_sem.at[0])
    pltpu.make_async_copy(wk_hbm, wkv.at[0], load_sem.at[1]).start()
    pltpu.make_async_copy(wv_hbm, wkv.at[1], load_sem.at[1]).start()
    load_kv = pltpu.make_async_copy(wkv, wkv, load_sem.at[1])
    load_wq = pltpu.make_async_copy(wq_hbm, wq, load_sem.at[2])
    load_wo = pltpu.make_async_copy(wo_hbm, wo, load_sem.at[3])
    load_wq.start()
    load_wo.start()

    barrier = pltpu.get_barrier_semaphore()
    pl.semaphore_signal(barrier, inc=1, device_id={"tp": sibling}, device_id_type=MESH)
    for step in range(1, pairs):
        pl.semaphore_signal(
            barrier, inc=1, device_id={"tp": far(step) * 2 + core}, device_id_type=MESH
        )
    pl.semaphore_signal(barrier, inc=1, device_id={"sp": side}, device_id_type=MESH)

    @pl.when(has_next)
    def _():
        pl.semaphore_signal(barrier, inc=1, device_id={"sp": sp + 2}, device_id_type=MESH)

    @pl.when(has_prev)
    def _():
        pl.semaphore_signal(barrier, inc=1, device_id={"sp": sp - 2}, device_id_type=MESH)

    pl.semaphore_wait(barrier, 1 + pairs + has_next.astype(jnp.int32) + has_prev.astype(jnp.int32))

    def tok_copy(slot, sem, recv, device):
        return pltpu.make_async_remote_copy(
            src_ref=slot,
            dst_ref=slot,
            send_sem=sem,
            recv_sem=recv,
            device_id={"tp": device},
            device_id_type=MESH,
        )

    def far_recv(step, role, h):
        return tok_recv.at[1 + ((step - 1) * 2 + role) * 2 + h]

    load_tok.wait()
    for h in range(2):
        for step in range(1, pairs):
            slot = tok.at[pair, core, h]
            goal = far(step) * 2 + core
            tok_copy(slot, tok_send.at[0], far_recv(step, 0, h), goal).start()
        if h == 0:
            tok_copy(tok.at[pair, core], tok_send.at[0], tok_recv.at[0], sibling).start()

    other = 1 - core
    cores = (core, other)

    def kv_at(block, step, role, h):
        chunk = near(step) if step else pair
        if step == 0:
            return kv.at[block, chunk, cores[role]], kv_recv.at[block, role]
        return (
            kv.at[block, chunk, cores[role], h],
            kv_recv.at[block, 2 + ((step - 1) * 2 + role) * 2 + h],
        )

    def kv_copy(slot, sem, recv, device):
        return pltpu.make_async_remote_copy(
            src_ref=slot,
            dst_ref=slot,
            send_sem=sem,
            recv_sem=recv,
            device_id={"sp": device},
            device_id_type=MESH,
        )

    def pass_on(d, step, role, h):
        block = sp - 2 * d
        slot, recv = kv_at(block, step, role, h)

        @pl.when(has_next)
        def _():
            kv_copy(slot, kv_next.at[d], recv, sp + 2).start()

        @pl.when(block < side)
        def _():
            kv_copy(slot, kv_side.at[d], recv, side).start()

    def sent(d):
        block = sp - 2 * d
        whole = kv.at[block]

        @pl.when(has_next)
        def _():
            kv_copy(whole, kv_next.at[d], kv_recv.at[0, 0], sp + 2).wait_send()

        @pl.when(block < side)
        def _():
            kv_copy(whole, kv_side.at[d], kv_recv.at[0, 0], side).wait_send()

    def arrived(block, step, role, h):
        slot, recv = kv_at(block, step, role, h)
        kv_copy(slot, kv_side.at[0], recv, side).wait_recv()

    def relay(d, step, role, h):
        arrived(sp - 2 * d, step, role, h)
        pass_on(d, step, role, h)

    def relay_near(d, role):
        @pl.when(d <= outer)
        def _():
            relay(d, 0, role, 0)

    def relay_far(d, role, h):
        @pl.when(d <= outer)
        def _():
            for step in range(1, pairs):
                relay(d, step, role, h)

    gain_t = jnp.broadcast_to(gain_ref[...], (count, VD)).T
    def project_near(role):
        c = cores[role]
        x = tok[pair, c].reshape(rows, depth)
        for s in range(2):
            made = jnp.dot(x, wkv[s], preferred_element_type=F32).astype(BF16)
            for h in range(2):
                kv[sp, pair, c, h, s] = made[h * half : (h + 1) * half]
        pass_on(0, 0, role, 0)

    def project_far(role, h):
        c = cores[role]
        for step in range(1, pairs):
            source = near(step)
            for s in range(2):
                kv[sp, source, c, h, s] = jnp.dot(
                    tok[source, c, h], wkv[s], preferred_element_type=F32
                ).astype(BF16)
            pass_on(0, step, role, h)

    def receive(role, h):
        for step in range(1, pairs):
            slot = tok.at[near(step), (core, other)[role], h]
            tok_copy(slot, tok_send.at[0], far_recv(step, role, h), sibling).wait_recv()

    def forward(h):
        receive(0, h)
        for step in range(1, pairs):
            slot = tok.at[near(step), core, h]
            tok_copy(slot, tok_send.at[1], far_recv(step, 1, h), sibling).start()

    load_kv.wait()
    project_near(0)
    tok_copy(tok.at[pair, other], tok_send.at[0], tok_recv.at[0], sibling).wait_recv()
    project_near(1)

    forward(0)
    project_far(0, 0)
    relay_near(1, 0)
    receive(1, 0)
    project_far(1, 0)
    relay_near(1, 1)
    forward(1)
    project_far(0, 1)
    receive(1, 1)
    project_far(1, 1)
    relay_near(2, 0)

    load_wq.wait()
    queries = jnp.dot(tok[...].reshape(count, depth), wq[...], preferred_element_type=F32)
    queries = queries.astype(BF16).astype(F32) * (1.0 / math.sqrt(QK))
    map_of = lax.broadcasted_iota(jnp.int32, (2 * QK, count), 0) // QK
    for g in range(groups):
        for k in range(2):
            at = (g * 2 + k) * 2 * QK
            turned = queries[:, at : at + 2 * QK].T
            for m in range(2):
                q_t[g, :, pl.ds((k * 2 + m) * count, count)] = jnp.where(
                    map_of == m, turned, 0.0
                ).astype(BF16)

    relay_far(1, 0, 0)
    relay_near(2, 1)
    relay_far(1, 1, 0)
    wide = 4 * count

    def absorb(block, first):
        for g in range(groups):
            lanes = slice(g * VD, (g + 1) * VD)
            keys = kv[block, :, :, :, 0, :, lanes].reshape(count, 2 * QK)
            values = kv[block, :, :, :, 1, :, lanes].reshape(count, VD)
            scores = jnp.dot(keys, q_t[g], preferred_element_type=F32)
            if first:
                key_at = lax.broadcasted_iota(jnp.int32, (count, wide), 0)
                query_at = lax.rem(lax.broadcasted_iota(jnp.int32, (count, wide), 1), count)
                scores = jnp.where(key_at <= query_at, scores, -jnp.inf)
            top = jnp.max(scores, axis=0, keepdims=True)
            if not first:
                old = peak[g]
                top = jnp.maximum(top, old)
                fade = jnp.exp(old - top)
            expo = jnp.exp(scores - top)
            amount = jnp.sum(expo, axis=0, keepdims=True)
            summed = lax.dot_general(
                values, expo.astype(BF16), (((0,), (0,)), ((), ())), preferred_element_type=F32
            )
            if not first:
                amount = amount + total[g] * fade
                summed = summed + acc[g] * fade
            peak[g] = top
            total[g] = amount
            acc[g] = summed

    absorb(sp, True)

    def turn(d, carried):
        for role in range(2):
            relay_near(d + 2, role)
        for role in range(2):
            relay_far(d + 1, role, 0)
        for role in range(2):
            relay_far(d, role, 1)
        absorb(sp - 2 * d, False)
        return carried

    lax.fori_loop(1, outer + 1, turn, 0)

    def beside(d, carried):
        block = side - 2 * d
        for role in range(2):
            arrived(block, 0, role, 0)
        for step in range(1, pairs):
            for h in range(2):
                for role in range(2):
                    arrived(block, step, role, h)
        absorb(block, False)
        return carried

    lax.fori_loop(1 - inner, outer + 1, beside, 0)

    for g in range(groups):
        for k in range(2):
            left = pl.ds((k * 2) * count, count)
            right = pl.ds((k * 2 + 1) * count, count)
            mixed = acc[g, :, left] / total[g, :, left] - lam_ref[g * 2 + k] * (
                acc[g, :, right] / total[g, :, right]
            )
            power = jnp.mean(mixed * mixed, axis=0, keepdims=True)
            head = mixed * lax.rsqrt(power + 1e-6) * gain_t
            heads[:, (g * 2 + k) * VD : (g * 2 + k + 1) * VD] = head.T.astype(BF16)

    load_wo.wait()

    def sib_copy(j):
        return pltpu.make_async_remote_copy(
            src_ref=part.at[j, 1 - core],
            dst_ref=from_sib.at[j],
            send_sem=out_send.at[0],
            recv_sem=sib_recv.at[j],
            device_id={"tp": sibling},
            device_id_type=MESH,
        )

    def pair_copy(j, step):
        return pltpu.make_async_remote_copy(
            src_ref=pair_out.at[j, step - 1],
            dst_ref=pair_in.at[j, step - 1],
            send_sem=out_send.at[1],
            recv_sem=pair_recv.at[j, step - 1],
            device_id={"tp": far(step) * 2 + core},
            device_id_type=MESH,
        )

    def out_sent(slots, kind):
        pltpu.make_async_remote_copy(
            src_ref=slots,
            dst_ref=slots,
            send_sem=out_send.at[kind],
            recv_sem=sib_recv.at[0],
            device_id={"tp": sibling},
            device_id_type=MESH,
        ).wait_send()

    for j in range(chunks):
        partial = jnp.dot(
            heads[...], wo[:, j * width : (j + 1) * width], preferred_element_type=F32
        ).astype(BF16)
        for p in range(pairs):
            for c in range(2):
                at = (p * 2 + c) * rows
                part[j, c, p] = partial[at : at + rows]
        sib_copy(j).start()
    for j in range(chunks):
        sib_copy(j).wait_recv()
        for step in range(1, pairs):
            goal = far(step)
            pair_out[j, step - 1] = (
                part[j, core, goal].astype(F32) + from_sib[j, goal].astype(F32)
            ).astype(BF16)
            pair_copy(j, step).start()
    tok_copy(tok.at[:, 0], tok_send.at[0], tok_recv.at[0], sibling).wait_send()
    fwd = tok.at[pl.ds(0, pairs - 1), 0]
    tok_copy(fwd, tok_send.at[1], tok_recv.at[0], sibling).wait_send()

    def drain(d, carried):
        sent(d)
        return carried

    lax.fori_loop(0, outer + 1, drain, 0)
    out_sent(part.at[:, 0], 0)
    for j in range(chunks):
        result = part[j, core, pair].astype(F32) + from_sib[j, pair].astype(F32)
        for step in range(1, pairs):
            pair_copy(j, step).wait_recv()
            result = result + pair_in[j, step - 1].astype(F32)
        out_ref[:, j * width : (j + 1) * width] = result.astype(BF16)

    out_sent(pair_out, 1)


def body(sp_size, tp_size, tokens, w_query, w_key, w_value, w_out, lambda_head, sub_gain):
    rows, depth = tokens.shape
    pairs = tp_size // 2
    count = rows * tp_size
    key_cols = w_key.shape[1]
    groups = key_cols // (2 * QK)
    out_cols = w_out.shape[1]
    chunks = math.gcd(out_cols // 128, 4)
    width = out_cols // chunks
    anywhere = pl.BlockSpec(memory_space=pl.ANY)
    dma = pltpu.SemaphoreType.DMA
    return pl.pallas_call(
        functools.partial(kernel, sp_size, tp_size),
        out_shape=pltpu.VMEM((rows, out_cols), BF16),
        in_specs=[anywhere] * 5
        + [pl.BlockSpec(memory_space=pltpu.SMEM), pl.BlockSpec(memory_space=pltpu.VMEM)],
        out_specs=pl.BlockSpec(memory_space=pltpu.VMEM),
        scratch_shapes=[
            pltpu.VMEM((pairs, 2, 2, rows // 2, depth), BF16),
            pltpu.VMEM(w_query.shape, BF16),
            pltpu.VMEM((2, *w_key.shape), BF16),
            pltpu.VMEM(w_out.shape, BF16),
            pltpu.VMEM((sp_size, pairs, 2, 2, 2, rows // 2, key_cols), BF16),
            pltpu.VMEM((groups, 2 * QK, 4 * count), BF16),
            pltpu.VMEM((groups, VD, 4 * count), F32),
            pltpu.VMEM((groups, 1, 4 * count), F32),
            pltpu.VMEM((groups, 1, 4 * count), F32),
            pltpu.VMEM((count, groups * 2 * VD), BF16),
            pltpu.VMEM((chunks, 2, pairs, rows, width), BF16),
            pltpu.VMEM((chunks, pairs, rows, width), BF16),
            pltpu.VMEM((chunks, pairs - 1, rows, width), BF16),
            pltpu.VMEM((chunks, pairs - 1, rows, width), BF16),
            dma((4,)),
            dma((2,)),
            dma((1 + 4 * (pairs - 1),)),
            dma(((sp_size + 1) // 2,)),
            dma(((sp_size + 1) // 2,)),
            dma((sp_size, 2 + 4 * (pairs - 1))),
            dma((2,)),
            dma((chunks,)),
            dma((chunks, pairs - 1)),
        ],
        compiler_params=pltpu.CompilerParams(
            collective_id=0, has_side_effects=True, vmem_limit_bytes=60 * 1024 * 1024
        ),
    )(tokens, w_query, w_key, w_value, w_out, lambda_head, sub_gain.reshape(1, VD))


def solution(mesh):
    return jax.shard_map(
        functools.partial(body, mesh.shape["sp"], mesh.shape["tp"]),
        mesh=mesh,
        in_specs=(
            P(("sp", "tp"), None),
            P(None, "tp"),
            P(None, "tp"),
            P(None, "tp"),
            P("tp", None),
            P("tp"),
            P(),
        ),
        out_specs=P(("sp", "tp"), None),
        check_vma=False,
    )
```

time: 28.7 us -> 27.9 us (0.972); the launches traced: 28.2 us -> 27.8 us
  Pallas kernels: 27.6 us -> 27.1 us
    pallas_call x1, Pallas kernels: 27.6 us -> 27.1 us  [body(): pl.pallas_call(functools.partial(kernel, sp_size, tp_size), out_shape=plt...]
where the time goes in v2:
time: 27.9 us; the launch traced here: 27.8 us
  Pallas kernels  27.1 us (97%)
  local copies, waits for them, and re-layouts  0.66 us (2%)
    pallas_call x1, Pallas kernels, body(): pl.pallas_call(functools.partial(kernel, sp_size, tp_size), out_shape=plt...  27.1 us
    unnamed x1, local copies, waits for them, and re-layouts  0.66 us

profile of v2, /device:TPU:25, one launch (start us, length us, event | category | flops | bytes accessed | tf_op | source)
XLA Modules:
  0.0 27.8 jit_solution(14747002127115951092)
XLA Ops:
  0.0 27.1 %shard_map.73 = bf16[32,2048]{1,0:T(8,128)(2,1)S(1)} custom-call(bf16[32,2048]{1,0:T(8,128)(2,1)} %tok_hbm.1, bf16[2048,512]{1,0:T(8,128)(2,1)} %wq_hbm.1, bf16[2048,256]{1,0:T(8,128)(2,1)} %wk_hbm.1, bf16[2048,256]{1,0:T(8,128)(2,1)} %wv_hbm.1, bf16[512,2048]{1,0:T(8,128)(2,1)} %wo_hbm.1, f32[4]{0:T(128)} %lam_ref.1, f32[1,128]{1,0:T(1,128)} %bitcast.1), custom_call_target="tpu_custom_call" | custom-call | tf_op jit(solution)/shard_map/pallas_call | solution.py:408
  27.1 0.7 %copy.9 = bf16[32,2048]{1,0:T(8,128)(2,1)} copy(bf16[32,2048]{1,0:T(8,128)(2,1)S(1)} %shard_map.73) | data formatting | bytes 262144

commit v3 on v2

--- a/solution.py
+++ b/solution.py
@@ -164,16 +164,16 @@
             kv_copy(slot, kv_side.at[d], recv, side).start()
 
     def sent(d):
-        block = sp - 2 * d
-        whole = kv.at[block]
+        whole = kv.at[sp - 2 * d]
+        recv = kv_recv.at[0, 0]
 
         @pl.when(has_next)
         def _():
-            kv_copy(whole, kv_next.at[d], kv_recv.at[0, 0], sp + 2).wait_send()
-
-        @pl.when(block < side)
-        def _():
-            kv_copy(whole, kv_side.at[d], kv_recv.at[0, 0], side).wait_send()
+            kv_copy(whole, kv_next.at[d], recv, sp + 2).wait_send()
+
+        @pl.when(sp - 2 * d < side)
+        def _():
+            kv_copy(whole, kv_side.at[d], recv, side).wait_send()
 
     def arrived(block, step, role, h):
         slot, recv = kv_at(block, step, role, h)
@@ -230,38 +230,26 @@
     tok_copy(tok.at[pair, other], tok_send.at[0], tok_recv.at[0], sibling).wait_recv()
     project_near(1)
 
-    forward(0)
-    project_far(0, 0)
-    relay_near(1, 0)
-    receive(1, 0)
-    project_far(1, 0)
-    relay_near(1, 1)
-    forward(1)
-    project_far(0, 1)
-    receive(1, 1)
-    project_far(1, 1)
-    relay_near(2, 0)
-
-    load_wq.wait()
-    queries = jnp.dot(tok[...].reshape(count, depth), wq[...], preferred_element_type=F32)
-    queries = queries.astype(BF16).astype(F32) * (1.0 / math.sqrt(QK))
     map_of = lax.broadcasted_iota(jnp.int32, (2 * QK, count), 0) // QK
-    for g in range(groups):
-        for k in range(2):
-            at = (g * 2 + k) * 2 * QK
-            turned = queries[:, at : at + 2 * QK].T
-            for m in range(2):
-                q_t[g, :, pl.ds((k * 2 + m) * count, count)] = jnp.where(
-                    map_of == m, turned, 0.0
-                ).astype(BF16)
-
-    relay_far(1, 0, 0)
-    relay_near(2, 1)
-    relay_far(1, 1, 0)
+
+    def ask(only):
+        for g in only:
+            span = slice(g * 4 * QK, (g + 1) * 4 * QK)
+            asked = jnp.dot(
+                tok[...].reshape(count, depth), wq[:, span], preferred_element_type=F32
+            )
+            asked = asked.astype(BF16).astype(F32) * (1.0 / math.sqrt(QK))
+            for k in range(2):
+                turned = asked[:, k * 2 * QK : (k + 1) * 2 * QK].T
+                for m in range(2):
+                    q_t[g, :, pl.ds((k * 2 + m) * count, count)] = jnp.where(
+                        map_of == m, turned, 0.0
+                    ).astype(BF16)
+
     wide = 4 * count
 
-    def absorb(block, first):
-        for g in range(groups):
+    def absorb(block, first, only=None):
+        for g in range(groups) if only is None else only:
             lanes = slice(g * VD, (g + 1) * VD)
             keys = kv[block, :, :, :, 0, :, lanes].reshape(count, 2 * QK)
             values = kv[block, :, :, :, 1, :, lanes].reshape(count, VD)
@@ -287,16 +275,37 @@
             total[g] = amount
             acc[g] = summed
 
-    absorb(sp, True)
+    relay_near(1, 0)
+    forward(0)
+    project_far(0, 0)
+    relay_near(1, 1)
+    receive(1, 0)
+    project_far(1, 0)
+    forward(1)
+    project_far(0, 1)
+    relay_near(2, 0)
+    receive(1, 1)
+    project_far(1, 1)
+    relay_near(2, 1)
+    relay_far(1, 0, 0)
+    relay_far(1, 1, 0)
+    load_wq.wait()
+    ask(range(groups // 2))
+    ask(range(groups // 2, groups))
+    absorb(sp, True, range(groups // 2))
+    relay_far(1, 0, 1)
+    absorb(sp, True, range(groups // 2, groups))
+    relay_far(1, 1, 1)
 
     def turn(d, carried):
-        for role in range(2):
-            relay_near(d + 2, role)
-        for role in range(2):
-            relay_far(d + 1, role, 0)
-        for role in range(2):
-            relay_far(d, role, 1)
-        absorb(sp - 2 * d, False)
+        relay_near(d + 2, 0)
+        relay_near(d + 2, 1)
+        relay_far(d + 1, 0, 0)
+        relay_far(d + 1, 1, 0)
+        absorb(sp - 2 * d, False, range(groups // 2))
+        relay_far(d + 1, 0, 1)
+        absorb(sp - 2 * d, False, range(groups // 2, groups))
+        relay_far(d + 1, 1, 1)
         return carried
 
     lax.fori_loop(1, outer + 1, turn, 0)
@@ -401,7 +410,7 @@
     key_cols = w_key.shape[1]
     groups = key_cols // (2 * QK)
     out_cols = w_out.shape[1]
-    chunks = math.gcd(out_cols // 128, 4)
+    chunks = math.gcd(out_cols // 128, 2)
     width = out_cols // chunks
     anywhere = pl.BlockSpec(memory_space=pl.ANY)
     dma = pltpu.SemaphoreType.DMA

time: 27.9 us -> 26.7 us (0.957)
  Pallas kernels: 27.1 us -> 25.8 us
    pallas_call x1, Pallas kernels: 27.1 us -> 25.8 us  [body(): pl.pallas_call(functools.partial(kernel, sp_size, tp_size), out_shape=plt...]
where the time goes in v3:
time: 26.7 us; the launch traced here: 26.5 us
  Pallas kernels  25.8 us (97%)
  local copies, waits for them, and re-layouts  0.66 us (2%)
    pallas_call x1, Pallas kernels, body(): pl.pallas_call(functools.partial(kernel, sp_size, tp_size), out_shape=plt...  25.8 us
    unnamed x1, local copies, waits for them, and re-layouts  0.66 us

profile of v3, /device:TPU:25, one launch (start us, length us, event | category | flops | bytes accessed | tf_op | source)
XLA Modules:
  0.0 26.5 jit_solution(11021550678375084664)
XLA Ops:
  0.0 25.8 %shard_map.73 = bf16[32,2048]{1,0:T(8,128)(2,1)S(1)} custom-call(bf16[32,2048]{1,0:T(8,128)(2,1)} %tok_hbm.1, bf16[2048,512]{1,0:T(8,128)(2,1)} %wq_hbm.1, bf16[2048,256]{1,0:T(8,128)(2,1)} %wk_hbm.1, bf16[2048,256]{1,0:T(8,128)(2,1)} %wv_hbm.1, bf16[512,2048]{1,0:T(8,128)(2,1)} %wo_hbm.1, f32[4]{0:T(128)} %lam_ref.1, f32[1,128]{1,0:T(1,128)} %bitcast.1), custom_call_target="tpu_custom_call" | custom-call | tf_op jit(solution)/shard_map/pallas_call | solution.py:417
  25.8 0.7 %copy.9 = bf16[32,2048]{1,0:T(8,128)(2,1)} copy(bf16[32,2048]{1,0:T(8,128)(2,1)S(1)} %shard_map.73) | data formatting | bytes 262144

commit v4 on v3

--- a/solution.py
+++ b/solution.py
@@ -13,6 +13,7 @@
 MESH = pl.DeviceIdType.MESH
 F32 = jnp.float32
 BF16 = jnp.bfloat16
+TURN = 2
 
 
 def kernel(
@@ -45,7 +46,9 @@
     tok_recv,
     kv_next,
     kv_side,
+    kv_diag,
     kv_recv,
+    ready,
     out_send,
     sib_recv,
     pair_recv,
@@ -132,6 +135,10 @@
     other = 1 - core
     cores = (core, other)
 
+    @pl.when(has_next)
+    def _():
+        pl.semaphore_signal(ready.at[0], inc=1, device_id={"sp": side}, device_id_type=MESH)
+
     def kv_at(block, step, role, h):
         chunk = near(step) if step else pair
         if step == 0:
@@ -154,26 +161,45 @@
     def pass_on(d, step, role, h):
         block = sp - 2 * d
         slot, recv = kv_at(block, step, role, h)
+        beside = block < side
 
         @pl.when(has_next)
         def _():
             kv_copy(slot, kv_next.at[d], recv, sp + 2).start()
 
-        @pl.when(block < side)
+        if step and h:
+            beside = jnp.logical_and(beside, d <= TURN)
+
+            @pl.when(jnp.logical_and(has_next, d >= TURN))
+            def _():
+                kv_copy(slot, kv_diag.at[d], recv, side + 2).start()
+
+        @pl.when(beside)
         def _():
             kv_copy(slot, kv_side.at[d], recv, side).start()
 
     def sent(d):
-        whole = kv.at[sp - 2 * d]
+        block = sp - 2 * d
+        whole = kv.at[block]
         recv = kv_recv.at[0, 0]
 
         @pl.when(has_next)
         def _():
             kv_copy(whole, kv_next.at[d], recv, sp + 2).wait_send()
 
-        @pl.when(sp - 2 * d < side)
+        @pl.when(jnp.logical_and(has_next, d >= TURN))
+        def _():
+            late = kv.at[block, pl.ds(0, pairs - 1), :, 0]
+            kv_copy(late, kv_diag.at[d], recv, side + 2).wait_send()
+
+        @pl.when(jnp.logical_and(block < side, d <= TURN))
         def _():
             kv_copy(whole, kv_side.at[d], recv, side).wait_send()
+
+        @pl.when(jnp.logical_and(block < side, d > TURN))
+        def _():
+            rest = kv.at[pl.ds(0, pairs + 1), 0, :, 0]
+            kv_copy(rest, kv_side.at[d], recv, side).wait_send()
 
     def arrived(block, step, role, h):
         slot, recv = kv_at(block, step, role, h)
@@ -283,6 +309,10 @@
     project_far(1, 0)
     forward(1)
     project_far(0, 1)
+    @pl.when(has_next)
+    def _():
+        pl.semaphore_wait(ready.at[0], 1)
+
     relay_near(2, 0)
     receive(1, 1)
     project_far(1, 1)
@@ -440,7 +470,9 @@
             dma((1 + 4 * (pairs - 1),)),
             dma(((sp_size + 1) // 2,)),
             dma(((sp_size + 1) // 2,)),
+            dma(((sp_size + 1) // 2,)),
             dma((sp_size, 2 + 4 * (pairs - 1))),
+            pltpu.SemaphoreType.REGULAR((1,)),
             dma((2,)),
             dma((chunks,)),
             dma((chunks, pairs - 1)),

time: 26.7 us -> 26.4 us (0.989)
  no operation moved by 1% of the time
where the time goes in v4:
time: 26.4 us; the launch traced here: 26.3 us
  Pallas kernels  25.6 us (97%)
  local copies, waits for them, and re-layouts  0.66 us (2%)
    pallas_call x1, Pallas kernels, body(): pl.pallas_call(functools.partial(kernel, sp_size, tp_size), out_shape=plt...  25.6 us
    unnamed x1, local copies, waits for them, and re-layouts  0.66 us

profile of v4, /device:TPU:25, one launch (start us, length us, event | category | flops | bytes accessed | tf_op | source)
XLA Modules:
  0.0 26.3 jit_solution(9821743846665435258)
XLA Ops:
  0.0 25.6 %shard_map.73 = bf16[32,2048]{1,0:T(8,128)(2,1)S(1)} custom-call(bf16[32,2048]{1,0:T(8,128)(2,1)} %tok_hbm.1, bf16[2048,512]{1,0:T(8,128)(2,1)} %wq_hbm.1, bf16[2048,256]{1,0:T(8,128)(2,1)} %wk_hbm.1, bf16[2048,256]{1,0:T(8,128)(2,1)} %wv_hbm.1, bf16[512,2048]{1,0:T(8,128)(2,1)} %wo_hbm.1, f32[4]{0:T(128)} %lam_ref.1, f32[1,128]{1,0:T(1,128)} %bitcast.1), custom_call_target="tpu_custom_call" | custom-call | tf_op jit(solution)/shard_map/pallas_call | solution.py:447
  25.6 0.7 %copy.9 = bf16[32,2048]{1,0:T(8,128)(2,1)} copy(bf16[32,2048]{1,0:T(8,128)(2,1)S(1)} %shard_map.73) | data formatting | bytes 262144

commit v5 on v4

--- a/solution.py
+++ b/solution.py
@@ -327,6 +327,16 @@
     absorb(sp, True, range(groups // 2, groups))
     relay_far(1, 1, 1)
 
+    def take_side(d):
+        block = side - 2 * d
+        for role in range(2):
+            arrived(block, 0, role, 0)
+        for step in range(1, pairs):
+            for h in range(2):
+                for role in range(2):
+                    arrived(block, step, role, h)
+        absorb(block, False)
+
     def turn(d, carried):
         relay_near(d + 2, 0)
         relay_near(d + 2, 1)
@@ -336,33 +346,31 @@
         relay_far(d + 1, 0, 1)
         absorb(sp - 2 * d, False, range(groups // 2, groups))
         relay_far(d + 1, 1, 1)
+
+        @pl.when(d - 1 >= 1 - inner)
+        def _():
+            take_side(d - 1)
+
         return carried
 
     lax.fori_loop(1, outer + 1, turn, 0)
 
     def beside(d, carried):
-        block = side - 2 * d
-        for role in range(2):
-            arrived(block, 0, role, 0)
-        for step in range(1, pairs):
-            for h in range(2):
-                for role in range(2):
-                    arrived(block, step, role, h)
-        absorb(block, False)
+        take_side(d)
         return carried
 
-    lax.fori_loop(1 - inner, outer + 1, beside, 0)
+    lax.fori_loop(jnp.maximum(1 - inner, outer - 0), outer + 1, beside, 0)
 
     for g in range(groups):
         for k in range(2):
             left = pl.ds((k * 2) * count, count)
             right = pl.ds((k * 2 + 1) * count, count)
-            mixed = acc[g, :, left] / total[g, :, left] - lam_ref[g * 2 + k] * (
-                acc[g, :, right] / total[g, :, right]
+            mixed = acc[g, :, left] * (1.0 / total[g, :, left]) - acc[g, :, right] * (
+                lam_ref[g * 2 + k] / total[g, :, right]
             )
             power = jnp.mean(mixed * mixed, axis=0, keepdims=True)
             head = mixed * lax.rsqrt(power + 1e-6) * gain_t
-            heads[:, (g * 2 + k) * VD : (g * 2 + k + 1) * VD] = head.T.astype(BF16)
+            heads[:, (g * 2 + k) * VD : (g * 2 + k + 1) * VD] = head.astype(BF16).T
 
     load_wo.wait()
 

time: 26.4 us -> 26.4 us (level)
  no operation moved by 1% of the time
where the time goes in v5:
time: 26.4 us; the launch traced here: 26.2 us
  Pallas kernels  25.6 us (97%)
  local copies, waits for them, and re-layouts  0.66 us (2%)
    pallas_call x1, Pallas kernels, body(): pl.pallas_call(functools.partial(kernel, sp_size, tp_size), out_shape=plt...  25.6 us
    unnamed x1, local copies, waits for them, and re-layouts  0.66 us

profile of v5, /device:TPU:25, one launch (start us, length us, event | category | flops | bytes accessed | tf_op | source)
XLA Modules:
  0.0 26.2 jit_solution(16439931302290162884)
XLA Ops:
  0.0 25.6 %shard_map.73 = bf16[32,2048]{1,0:T(8,128)(2,1)S(1)} custom-call(bf16[32,2048]{1,0:T(8,128)(2,1)} %tok_hbm.1, bf16[2048,512]{1,0:T(8,128)(2,1)} %wq_hbm.1, bf16[2048,256]{1,0:T(8,128)(2,1)} %wk_hbm.1, bf16[2048,256]{1,0:T(8,128)(2,1)} %wv_hbm.1, bf16[512,2048]{1,0:T(8,128)(2,1)} %wo_hbm.1, f32[4]{0:T(128)} %lam_ref.1, f32[1,128]{1,0:T(1,128)} %bitcast.1), custom_call_target="tpu_custom_call" | custom-call | tf_op jit(solution)/shard_map/pallas_call | solution.py:455
  25.6 0.7 %copy.9 = bf16[32,2048]{1,0:T(8,128)(2,1)} copy(bf16[32,2048]{1,0:T(8,128)(2,1)S(1)} %shard_map.73) | data formatting | bytes 262144

commit v6 on v5

--- a/solution.py
+++ b/solution.py
@@ -89,8 +89,6 @@
     load_kv = pltpu.make_async_copy(wkv, wkv, load_sem.at[1])
     load_wq = pltpu.make_async_copy(wq_hbm, wq, load_sem.at[2])
     load_wo = pltpu.make_async_copy(wo_hbm, wo, load_sem.at[3])
-    load_wq.start()
-    load_wo.start()
 
     barrier = pltpu.get_barrier_semaphore()
     pl.semaphore_signal(barrier, inc=1, device_id={"tp": sibling}, device_id_type=MESH)
@@ -252,6 +250,8 @@
             tok_copy(slot, tok_send.at[1], far_recv(step, 1, h), sibling).start()
 
     load_kv.wait()
+    load_wq.start()
+    load_wo.start()
     project_near(0)
     tok_copy(tok.at[pair, other], tok_send.at[0], tok_recv.at[0], sibling).wait_recv()
     project_near(1)

time: 26.4 us -> 26.4 us (level)
  no operation moved by 1% of the time
where the time goes in v6:
time: 26.4 us; the launch traced here: 26.2 us
  Pallas kernels  25.6 us (97%)
  local copies, waits for them, and re-layouts  0.66 us (2%)
    pallas_call x1, Pallas kernels, body(): pl.pallas_call(functools.partial(kernel, sp_size, tp_size), out_shape=plt...  25.6 us
    unnamed x1, local copies, waits for them, and re-layouts  0.66 us

profile of v6, /device:TPU:25, one launch (start us, length us, event | category | flops | bytes accessed | tf_op | source)
XLA Modules:
  0.0 26.2 jit_solution(7857942081565686506)
XLA Ops:
  0.0 25.6 %shard_map.73 = bf16[32,2048]{1,0:T(8,128)(2,1)S(1)} custom-call(bf16[32,2048]{1,0:T(8,128)(2,1)} %tok_hbm.1, bf16[2048,512]{1,0:T(8,128)(2,1)} %wq_hbm.1, bf16[2048,256]{1,0:T(8,128)(2,1)} %wk_hbm.1, bf16[2048,256]{1,0:T(8,128)(2,1)} %wv_hbm.1, bf16[512,2048]{1,0:T(8,128)(2,1)} %wo_hbm.1, f32[4]{0:T(128)} %lam_ref.1, f32[1,128]{1,0:T(1,128)} %bitcast.1), custom_call_target="tpu_custom_call" | custom-call | tf_op jit(solution)/shard_map/pallas_call | solution.py:455
  25.6 0.7 %copy.9 = bf16[32,2048]{1,0:T(8,128)(2,1)} copy(bf16[32,2048]{1,0:T(8,128)(2,1)S(1)} %shard_map.73) | data formatting | bytes 262144
